TPU v7x, 32 devices: a whole 2x2x4 slice. The times are simulated.
32 devices in a mesh: grp: 2 (over y), fs: 4 (over z), tp: 4 (over x, core).
Axes of the slice: x: 2, y: 2, z: 4, core: 2. Of those that a mesh axis runs over, the one named last changes fastest.
Arguments:
- tokens: bfloat16 [8, 1024, 2048], P(('grp', 'fs'), None, 'tp'), parts along dimension 0, may hold values from -6 to 6
- mix_gain: float32 [2048], replicated, may hold values from 0.1 to 1.9
- in_matrix: float32 [2048, 1024], P('fs', 'tp'), may hold values from -0.125 to 0.125
- in_scale: float32 [1, 1024], P(None, 'tp'), may hold values from 0.5 to 2
- pool_mix: bfloat16 [8, 128, 128], P('tp'), may hold values from -0.5 to 0.5
- pool_scale: float32 [1, 1024], P(None, 'tp'), may hold values from 0.1 to 1.9
- out_matrix: float32 [1024, 2048], P('tp', 'fs'), may hold values from -0.25 to 0.25
- out_scale: float32 [1, 2048], P(None, 'fs'), may hold values from 0.5 to 2
- ffn_gain: float32 [2048], replicated, may hold values from 0.1 to 1.9
- gate_matrix: float32 [2048, 5632], P('fs', 'tp'), may hold values from -0.125 to 0.125
- gate_scale: float32 [1, 5632], P(None, 'tp'), may hold values from 0.5 to 2
- up_matrix: float32 [2048, 5632], P('fs', 'tp'), may hold values from -0.125 to 0.125
- up_scale: float32 [1, 5632], P(None, 'tp'), may hold values from 0.5 to 2
- gate_taps: float32 [3, 5632], P(None, 'tp'), may hold values from -4 to 4
- up_taps: float32 [3, 5632], P(None, 'tp'), may hold values from -4 to 4
- down_matrix: float32 [5632, 2048], P('tp', 'fs'), may hold values from -0.109375 to 0.109375
- down_scale: float32 [1, 2048], P(None, 'fs'), may hold values from 0.5 to 2
Outputs:
- layer_out: bfloat16 [8, 1024, 2048], P(('grp', 'fs'), None, 'tp'), parts along dimension 0
There are 2 independent parts, one for each index of `grp`. A program takes and returns all parts, laid end to end along the dimension named above; an argument that names none is the same for every part. Nothing has to cross between parts.
All inputs are finite; a program needn't handle non-finite values.
Results may differ from a plain program's by a relative error of at most 0.025.
Values may be sent and summed in bfloat16 or wider, within the bound.
No kernel may reach another device: no remote copies, remote signals or barrier semaphores. Data moves between devices by JAX's collectives and lax.ppermute only.
A program may use at most 128 MiB of HBM per device.

v0:
```python
import jax
import jax.numpy as jnp
from jax import lax
from jax.sharding import PartitionSpec as P

BLOCKS = 8
eps = 1e-06
widest_span = 16


def norm_rows(tok_rows, norm_gain):
    values = tok_rows.astype(jnp.float32)
    scaled = values * lax.rsqrt(jnp.mean(values * values, axis=-1, keepdims=True) + eps)
    return (scaled * norm_gain).astype(jnp.bfloat16)


def span_widths(block_ids):
    return jnp.left_shift(jnp.ones_like(block_ids), 1 + 4 * block_ids // BLOCKS)


def trailing_gap(projected, windows):
    values = projected.astype(jnp.float32)
    length = values.shape[0]
    running = values
    for offset in range(1, widest_span):
        shifted = jnp.pad(values[: length - offset], ((offset, 0), (0, 0)))
        running = running + jnp.where(windows[None, :] > offset, shifted, jnp.zeros_like(shifted))
    positions = jnp.arange(length, dtype=jnp.int32)[:, None]
    counts = jnp.minimum(positions + 1, windows[None, :]).astype(jnp.float32)
    return (running / counts - values).astype(jnp.bfloat16)


def causal_taps(linear, tap_table):
    values = linear.astype(jnp.float32)
    length = values.shape[0]
    back_one = jnp.pad(values[: length - 1], ((1, 0), (0, 0)))
    back_two = jnp.pad(values[: length - 2], ((2, 0), (0, 0)))
    return tap_table[2] * values + tap_table[1] * back_one + tap_table[0] * back_two


def fold_rows(operand, portion):
    return jnp.dot(operand, portion, preferred_element_type=jnp.float32)


def shards(
    tokens,
    mix_gain,
    in_matrix,
    in_scale,
    pool_mix,
    pool_scale,
    out_matrix,
    out_scale,
    ffn_gain,
    gate_matrix,
    gate_scale,
    up_matrix,
    up_scale,
    gate_taps,
    up_taps,
    down_matrix,
    down_scale,
):
    length = tokens.shape[1]
    own_width = tokens.shape[2]
    local_rows = tokens.reshape(length, own_width)
    gathered = lax.all_gather(local_rows, "tp", axis=1, tiled=True)
    normed = norm_rows(gathered, mix_gain)
    width_in = in_matrix.shape[1]
    in_total = fold_rows(
        normed, lax.all_gather(in_matrix.astype(jnp.bfloat16), "fs", axis=0, tiled=True)
    )
    projected = (in_total * in_scale).astype(jnp.bfloat16)
    local_blocks = pool_mix.shape[0]
    block_width = pool_mix.shape[1]
    block_ids = lax.axis_index("tp") * local_blocks + jnp.arange(local_blocks, dtype=jnp.int32)
    windows = jnp.repeat(span_widths(block_ids), block_width)
    spread = trailing_gap(projected, windows)
    block_mixed = jnp.einsum(
        "lbc,bce->lbe",
        spread.reshape(length, local_blocks, block_width),
        pool_mix,
        preferred_element_type=jnp.float32,
    ).reshape(length, width_in)
    pooled = (block_mixed * pool_scale).astype(jnp.bfloat16)
    out_cols = lax.all_gather(out_scale, "fs", axis=1, tiled=True)
    tp_index = lax.axis_index("tp")
    groups = lax.axis_size("tp")
    pooled_all = lax.all_gather(pooled, "tp", axis=1, tiled=True)
    row_block = lax.all_gather(out_matrix.astype(jnp.bfloat16), "fs", axis=1, tiled=True)
    own_matrix = lax.all_to_all(row_block, "tp", split_axis=1, concat_axis=0, tiled=True)
    own_scales = lax.dynamic_slice_in_dim(out_cols, tp_index * own_width, own_width, 1)
    grouped_rows = pooled_all.reshape(length, groups, width_in)
    grouped_matrix = own_matrix.reshape(groups, width_in, own_width)
    pieces = (
        jnp.einsum("lgc,gcd->gld", grouped_rows, grouped_matrix, preferred_element_type=jnp.float32)
        * own_scales[None]
    )
    rounded = lax.optimization_barrier(pieces.astype(jnp.bfloat16))
    mixing = jnp.sum(rounded.astype(jnp.float32), axis=0)
    residual = (local_rows.astype(jnp.float32) + mixing).astype(jnp.bfloat16)
    gathered_ffn = lax.all_gather(residual, "tp", axis=1, tiled=True)
    normed_ffn = norm_rows(gathered_ffn, ffn_gain)
    gate_cast = gate_matrix.astype(jnp.bfloat16)
    up_cast = up_matrix.astype(jnp.bfloat16)
    gate_full, up_full = (
        lax.all_gather(gate_cast, "fs", axis=0, tiled=True),
        lax.all_gather(up_cast, "fs", axis=0, tiled=True),
    )
    gate_total = jnp.dot(normed_ffn, gate_full, preferred_element_type=jnp.float32)
    up_total = jnp.dot(normed_ffn, up_full, preferred_element_type=jnp.float32)
    gate_lin = (gate_total * gate_scale).astype(jnp.bfloat16)
    up_lin = (up_total * up_scale).astype(jnp.bfloat16)
    hidden = (jax.nn.silu(causal_taps(gate_lin, gate_taps)) * causal_taps(up_lin, up_taps)).astype(
        jnp.bfloat16
    )
    down_cols = lax.all_gather(down_scale, "fs", axis=1, tiled=True)
    partial_ffn = (
        jnp.dot(
            hidden,
            lax.all_gather(down_matrix.astype(jnp.bfloat16), "fs", axis=1, tiled=True),
            preferred_element_type=jnp.float32,
        )
        * down_cols
    )
    feed_out = lax.psum_scatter(
        partial_ffn.astype(jnp.bfloat16), "tp", scatter_dimension=1, tiled=True
    ).astype(jnp.float32)
    result = (residual.astype(jnp.float32) + feed_out).astype(jnp.bfloat16)
    return result.reshape(1, length, result.shape[1])


def solution(mesh):
    return jax.shard_map(
        shards,
        mesh=mesh,
        in_specs=(
            P(("grp", "fs"), None, "tp"),
            P(),
            P("fs", "tp"),
            P(None, "tp"),
            P("tp", None, None),
            P(None, "tp"),
            P("tp", "fs"),
            P(None, "fs"),
            P(),
            P("fs", "tp"),
            P(None, "tp"),
            P("fs", "tp"),
            P(None, "tp"),
            P(None, "tp"),
            P(None, "tp"),
            P("tp", "fs"),
            P(None, "fs"),
        ),
        out_specs=P(("grp", "fs"), None, "tp"),
        check_vma=False,
    )
```

profile of v0, /device:TPU:0, one launch (start us, length us, event | category | flops | bytes accessed | tf_op | source)
XLA Modules:
  0.0 573.4 jit_solution(17679194408588764987)
XLA Ops:
  11.3 34.8 %all-gather.24.cloned.1.call-done = bf16[1,1024,2048]{2,1,0:T(8,128)(2,1)} async-done(((bf16[1,1024,512]{2,1,0:T(8,128)(2,1)}), bf16[1,1024,2048]{2,1,0:T(8,128)(2,1)}) %all-gather.24.cloned.1.call-update) | async-done | bytes 4194320 | tf_op jit(solution)/shard_map/all_gather | solution.py:67
  46.1 3.1 fusion.3
  49.2 26.5 %all-gather.10.cloned.1.call-done = bf16[2048,256]{1,0:T(8,128)(2,1)} async-done(((bf16[512,256]{1,0:T(8,128)(2,1)}), bf16[2048,256]{1,0:T(8,128)(2,1)}) %all-gather.10.cloned.1.call-update) | async-done | bytes 1048592 | tf_op jit(solution)/shard_map/all_gather | solution.py:71
  75.7 3.8 fusion.20
  80.1 3.2 fusion.28
  84.3 20.3 %all-gather.14.cloned.1.call-done = bf16[256,2048]{0,1:T(8,128)(2,1)} async-done(((bf16[256,512]{0,1:T(8,128)(2,1)}), bf16[256,2048]{0,1:T(8,128)(2,1)}) %all-gather.14.cloned.1.call-update) | async-done | bytes 1048592 | tf_op jit(solution)/shard_map/all_gather | solution.py:90
  104.7 2.3 copy.23
  106.9 3.5 all-to-all-start
  110.5 11.9 %all_gather.34 = f32[1,2048]{1,0:T(1,128)S(1)} all-gather(f32[1,512]{1,0:T(1,128)S(1)} %copy-done.10), channel_id=1, replica_groups=mesh['grp'=2,'fs'=4,'tp'=4] {'fs'}, dimensions={1}, use_global_device_ids=true | all-gather | bytes 10240 | tf_op jit(solution)/shard_map/all_gather | solution.py:86
  122.5 12.5 %all-to-all-done = bf16[256,4,512]{2,0,1:T(8,128)(2,1)S(1)} async-done(((bf16[256,4,512]{2,0,1:T(8,128)(2,1)}), bf16[256,4,512]{2,0,1:T(8,128)(2,1)S(1)}, u32[]{:S(2)}, u32[]{:S(2)}) %all-to-all-start) | async-done | bytes 1048608 | tf_op jit(solution)/shard_map/all_to_all | solution.py:91
  135.0 2.7 all-gather.12.cloned.1.call-done
  137.6 3.0 multiply_convert_fusion.1
  144.2 3.3 convert_element_type.136
  149.0 12.1 %all_gather.39 = f32[1,2048]{1,0:T(1,128)S(1)} all-gather(f32[1,512]{1,0:T(1,128)S(1)} %copy-done.11), channel_id=1, replica_groups=mesh['grp'=2,'fs'=4,'tp'=4] {'fs'}, dimensions={1}, use_global_device_ids=true | all-gather | bytes 10240 | tf_op jit(solution)/shard_map/all_gather | solution.py:117
  161.2 14.5 %all-gather.16.cloned.1.call-done = bf16[1024,2048]{1,0:T(8,128)(2,1)} async-done(((bf16[1024,512]{1,0:T(8,128)(2,1)}), bf16[1024,2048]{1,0:T(8,128)(2,1)}) %all-gather.16.cloned.1.call-update) | async-done | bytes 4194320 | tf_op jit(solution)/shard_map/all_gather | solution.py:102
  175.7 3.1 fusion
  178.8 105.1 %all-gather.18.cloned.1.call-done = bf16[2048,1408]{1,0:T(8,128)(2,1)} async-done(((bf16[512,1408]{1,0:T(8,128)(2,1)}), bf16[2048,1408]{1,0:T(8,128)(2,1)}) %all-gather.18.cloned.1.call-update) | async-done | bytes 5767184 | tf_op jit(solution)/shard_map/all_gather | solution.py:107
  283.9 11.9 %fusion.11 = f32[1024,1408]{1,0:T(8,128)} fusion(bf16[2048,1408]{1,0:T(8,128)(2,1)} %all-gather.18.cloned.1.call-done, f32[1408]{0:T(1024)S(1)} %reduce.1, bf16[1024,2048]{1,0:T(8,128)(2,1)} %all-gather.16.cloned.1.call-done, f32[2048]{0:T(1024)S(1)} %copy-done.14, f32[1024]{0:T(1024)S(1)} %add_rsqrt_fusion), kind=kOutput, calls=%fused_computation.20 | convolution fusion | flops 5918294016 | bytes 15746560 | tf_op jit(solution)/shard_map/dot_general | solution.py:110
  295.8 94.7 %all-gather.20.cloned.1.call-done = bf16[2048,1408]{1,0:T(8,128)(2,1)} async-done(((bf16[512,1408]{1,0:T(8,128)(2,1)}), bf16[2048,1408]{1,0:T(8,128)(2,1)}) %all-gather.20.cloned.1.call-update) | async-done | bytes 5767184 | tf_op jit(solution)/shard_map/all_gather | solution.py:108
  390.4 12.0 %fusion.12 = f32[1024,1408]{1,0:T(8,128)} fusion(bf16[2048,1408]{1,0:T(8,128)(2,1)} %all-gather.20.cloned.1.call-done, f32[1408]{0:T(1024)S(1)} %reduce.5, bf16[1024,2048]{1,0:T(8,128)(2,1)} %all-gather.16.cloned.1.call-done, f32[2048]{0:T(1024)S(1)} %copy-done.14, f32[1024]{0:T(1024)S(1)} %add_rsqrt_fusion), kind=kOutput, calls=%fused_computation.21 | convolution fusion | flops 5918294016 | bytes 15746560 | tf_op jit(solution)/shard_map/dot_general | solution.py:111
  402.4 94.6 %all-gather.22.cloned.1.call-done = bf16[1408,2048]{1,0:T(8,128)(2,1)} async-done(((bf16[1408,512]{1,0:T(8,128)(2,1)}), bf16[1408,2048]{1,0:T(8,128)(2,1)}) %all-gather.22.cloned.1.call-update) | async-done | bytes 5767184 | tf_op jit(solution)/shard_map/all_gather | solution.py:121
  497.0 24.6 %multiply_convert_fusion = bf16[1024,2048]{1,0:T(8,128)(2,1)} fusion(bf16[1408,2048]{1,0:T(8,128)(2,1)} %all-gather.22.cloned.1.call-done, f32[2048]{0:T(1024)S(1)} %bitcast.83, f32[1022,1408]{1,0:T(8,128)} %bitcast.89, f32[1023,1408]{1,0:T(8,128)} %bitcast.90, f32[1024,1408]{1,0:T(8,128)} %fusion.12, f32[1022,1408]{1,0:T(8,128)} %bitcast.87, ...), kind=kOutput, calls=%fused_computation.10 | convolution fusion | flops 5932843008 | bytes 44572672 | tf_op jit(solution)/shard_map/dot_general | solution.py:119
  521.6 42.8 %reduce-scatter.2.cloned.1.call-done = bf16[1024,512]{1,0:T(8,128)(2,1)} async-done(((bf16[1024,2048]{1,0:T(8,128)(2,1)}), bf16[1024,512]{1,0:T(8,128)(2,1)}) %reduce-scatter.2.cloned.1.call-update) | async-done | bytes 1048592 | tf_op jit(solution)/shard_map/reduce_scatter | solution.py:126
  564.4 2.5 fusion.25
  (75 shorter events, 11.3 us)
Async XLA Ops:
  6.5 73.6 %copy-start = (bf16[2,128,128]{2,1,0:T(8,128)(2,1)S(1)}, bf16[2,128,128]{2,1,0:T(8,128)(2,1)}, u32[]{:S(2)}) copy-start(bf16[2,128,128]{2,1,0:T(8,128)(2,1)} %param.21) | copy-start | bytes 196612
  6.5 69.2 %copy-start.15 = (f32[1,256]{1,0:T(1,128)S(1)}, f32[1,256]{1,0:T(1,128)}, u32[]{:S(2)}) copy-start(f32[1,256]{1,0:T(1,128)} %param.20) | copy-start | bytes 3076
  6.5 69.2 %copy-start.13 = (f32[2048]{0:T(1024)S(1)}, f32[2048]{0:T(1024)}, u32[]{:S(2)}) copy-start(f32[2048]{0:T(1024)} %param.18) | copy-start | bytes 24580
  6.5 39.6 %all-gather.24.cloned.1.call-start = ((), (), s32[]{:S(2)}) async-start(), calls=%async_computation.10 | async-start | bytes 5242880 | tf_op jit(solution)/shard_map/all_gather | solution.py:67
  7.3 68.4 %all-gather.10.cloned.1.call-start = ((), (), s32[]{:S(2)}) async-start(), calls=%async_computation.2 | async-start | bytes 1310720 | tf_op jit(solution)/shard_map/all_gather | solution.py:71
  9.1 95.6 %all-gather.14.cloned.1.call-start = ((), (), s32[]{:S(2)}) async-start(), calls=%async_computation.4 | async-start | bytes 1310720 | tf_op jit(solution)/shard_map/all_gather | solution.py:90
  11.1 126.6 %all-gather.12.cloned.1.call-start = ((), (), s32[]{:S(2)}) async-start(), calls=%async_computation.3 | async-start | bytes 2621440 | tf_op jit(solution)/shard_map/all_gather | solution.py:89
  83.4 27.1 %copy-start.10 = (f32[1,512]{1,0:T(1,128)S(1)}, f32[1,512]{1,0:T(1,128)}, u32[]{:S(2)}) copy-start(f32[1,512]{1,0:T(1,128)} %param.24) | copy-start | bytes 6148
  106.9 28.0 %all-to-all-start = ((bf16[256,4,512]{2,0,1:T(8,128)(2,1)}), bf16[256,4,512]{2,0,1:T(8,128)(2,1)S(1)}, u32[]{:S(2)}, u32[]{:S(2)}) async-start(bf16[256,4,512]{2,0,1:T(8,128)(2,1)} %copy.23), calls=%async_computation | async-start | bytes 2097152 | tf_op jit(solution)/shard_map/all_to_all | solution.py:91
  110.5 65.3 %all-gather.16.cloned.1.call-start = ((), (), s32[]{:S(2)}) async-start(), calls=%async_computation.5 | async-start | bytes 5242880 | tf_op jit(solution)/shard_map/all_gather | solution.py:102
  137.6 3.7 copy-start.3
  142.7 141.2 %all-gather.18.cloned.1.call-start = ((), (), s32[]{:S(2)}) async-start(), calls=%async_computation.6 | async-start | bytes 7208960 | tf_op jit(solution)/shard_map/all_gather | solution.py:107
  144.0 3.5 copy-start.5
  144.1 4.8 copy-start.8
  144.1 4.9 copy-start.9
  144.1 4.9 copy-start.11
  144.1 17.0 %copy-start.6 = (f32[3,1408]{1,0:T(4,128)S(1)}, f32[3,1408]{1,0:T(4,128)}, u32[]{:S(2)}) copy-start(f32[3,1408]{1,0:T(4,128)} %param.31) | copy-start | bytes 50692
  144.1 17.0 %copy-start.7 = (f32[3,1408]{1,0:T(4,128)S(1)}, f32[3,1408]{1,0:T(4,128)}, u32[]{:S(2)}) copy-start(f32[3,1408]{1,0:T(4,128)} %param.30) | copy-start | bytes 50692
  144.1 246.3 %all-gather.20.cloned.1.call-start = ((), (), s32[]{:S(2)}) async-start(), calls=%async_computation.7 | async-start | bytes 7208960 | tf_op jit(solution)/shard_map/all_gather | solution.py:108
  147.5 136.4 %copy-start.14 = (f32[2048]{0:T(1024)S(1)}, f32[2048]{0:T(1024)}, u32[]{:S(2)}) copy-start(f32[2048]{0:T(1024)} %param.25) | copy-start | bytes 24580
  147.5 349.5 %all-gather.22.cloned.1.call-start = ((), (), s32[]{:S(2)}) async-start(), calls=%async_computation.8 | async-start | bytes 7208960 | tf_op jit(solution)/shard_map/all_gather | solution.py:121
  148.8 415.6 %reduce-scatter.2.cloned.1.call-start = ((), (), s32[]{:S(2)}) async-start(), calls=%async_computation.9 | async-start | bytes 5242880 | tf_op jit(solution)/shard_map/reduce_scatter | solution.py:126
  497.0 67.4 %copy-start.2 = (bf16[1024,512]{1,0:T(8,128)(2,1)S(1)}, bf16[1024,512]{1,0:T(8,128)(2,1)}, u32[]{:S(2)}) copy-start(bf16[1024,512]{1,0:T(8,128)(2,1)} %fusion.13) | copy-start | bytes 3145732
  497.0 69.9 %copy-start.1 = (bf16[2,128,128]{2,1,0:T(8,128)(2,1)S(1)}, bf16[2,128,128]{2,1,0:T(8,128)(2,1)}, u32[]{:S(2)}) copy-start(bf16[2,128,128]{2,1,0:T(8,128)(2,1)} %param.21) | copy-start | bytes 196612
  (2 other events, 5.4 us)
Sparse Core Ops, SparseCore 0:
  8.9 37.1 all-gather.23
  47.7 27.9 all-gather.9
  77.3 27.3 all-gather.13
  106.1 31.4 all-gather.11
  142.8 32.9 all-gather.15
  177.2 106.6 all-gather.17
  285.5 104.9 all-gather.19
  392.0 104.9 all-gather.21
  521.8 42.6 reduce-scatter.1
where the time goes:
time: 574 us; the launch traced here: 573 us
  waiting for transfers between devices  449 us (78%)
  matrix products  58.5 us (10%)
  blocking collectives  24.1 us (4%)
  other arithmetic  19.3 us (3%)
  between operations  13.5 us (2%)
    all_gather x1, waiting for transfers between devices, shards(): lax.all_gather(gate_cast, 'fs', axis=0, tiled=True)  105 us
    all_gather x1, waiting for transfers between devices, shards(): lax.all_gather(up_cast, 'fs', axis=0, tiled=True)  94.7 us
    all_gather x1, waiting for transfers between devices, shards(): lax.all_gather(down_matrix.astype(jnp.bfloat16), 'fs', axis=1, tiled=True)  94.6 us
    reduce_scatter x1, waiting for transfers between devices, shards(): lax.psum_scatter(partial_ffn.astype(jnp.bfloat16), 'tp', scatter_dimensio...  42.8 us
    all_gather x1, waiting for transfers between devices, shards(): gathered = lax.all_gather(local_rows, 'tp', axis=1, tiled=True)  34.8 us
    all_gather x1, waiting for transfers between devices, shards(): lax.all_gather(in_matrix.astype(jnp.bfloat16), 'fs', axis=0, tiled=True)  26.5 us
    dot_general x1, matrix products, shards(): jnp.dot(hidden, lax.all_gather(down_matrix.astype(jnp.bfloat16), 'fs', ax...  24.6 us
    all_gather x1, waiting for transfers between devices, shards(): lax.all_gather(out_matrix.astype(jnp.bfloat16), 'fs', axis=1, tiled=True)  20.3 us
  transfers between devices with their start and end apart: 10, of which 10 were waited for; matrix products, arithmetic and copies ran while one was open for 9% of the time, Pallas kernels for 0%

commit v1 on v0

--- a/solution.py
+++ b/solution.py
@@ -6,6 +6,23 @@
 BLOCKS = 8
 eps = 1e-06
 widest_span = 16
+
+
+def laid_out(tiles, dim):
+    shape = list(tiles.shape[1:])
+    shape[dim] *= tiles.shape[0]
+    return jnp.moveaxis(tiles, 0, dim).reshape(shape)
+
+
+def ring_gather(x, axis, dim):
+    length = lax.axis_size(axis)
+    right = [(i, (i + 1) % length) for i in range(length)]
+    blocks = [x]
+    while len(blocks) < length:
+        blocks.append(lax.ppermute(blocks[-1], axis, right))
+    here = lax.axis_index(axis)
+    blocks = jnp.stack(blocks)[(here - jnp.arange(length)) % length]
+    return laid_out(blocks, dim)
 
 
 def norm_rows(tok_rows, norm_gain):
@@ -105,7 +122,7 @@
     up_cast = up_matrix.astype(jnp.bfloat16)
     gate_full, up_full = (
         lax.all_gather(gate_cast, "fs", axis=0, tiled=True),
-        lax.all_gather(up_cast, "fs", axis=0, tiled=True),
+        ring_gather(up_cast, "fs", 0),
     )
     gate_total = jnp.dot(normed_ffn, gate_full, preferred_element_type=jnp.float32)
     up_total = jnp.dot(normed_ffn, up_full, preferred_element_type=jnp.float32)

time: 574 us -> 524 us (0.913)
  waiting for transfers between devices: 449 us -> 302 us
  blocking collectives: 24.1 us -> 86.9 us
  starting transfers between devices: 3.85 us -> 27.7 us
  local copies, waits for them, and re-layouts: 4.94 us -> 11.6 us
  other arithmetic: 19.3 us -> 25.3 us
    all_gather x1, waiting for transfers between devices: 105 us -> 0.02 us  [shards(): lax.all_gather(gate_cast, 'fs', axis=0, tiled=True)]
    ppermute x0 -> x3, waiting for transfers between devices: none -> 97.1 us  [ring_gather(): blocks.append(lax.ppermute(blocks[-1], axis, right))]
    all_gather x1 -> x0, waiting for transfers between devices: 94.7 us -> none  [shards(): lax.all_gather(up_cast, 'fs', axis=0, tiled=True)]
    all_gather x1, blocking collectives: 12.1 us -> 74.9 us  [shards(): down_cols = lax.all_gather(down_scale, 'fs', axis=1, tiled=True)]
    all_gather x1, waiting for transfers between devices: 94.6 us -> 64.5 us  [shards(): lax.all_gather(down_matrix.astype(jnp.bfloat16), 'fs', axis=1, tiled=True)]
    ppermute x0 -> x3, starting transfers between devices: none -> 23.9 us  [ring_gather(): blocks.append(lax.ppermute(blocks[-1], axis, right))]
    all_gather x1, waiting for transfers between devices: 14.5 us -> 0.01 us  [shards(): gathered_ffn = lax.all_gather(residual, 'tp', axis=1, tiled=True)]
    gather x0 -> x1, local copies, waits for them, and re-layouts: none -> 6.67 us  [ring_gather(): blocks = jnp.stack(blocks)[(here - jnp.arange(length)) % length]]
  transfers between devices with their start and end apart: 10 -> 12, of which waited for: 10 -> 9; matrix products, arithmetic and copies ran while one was open for 9% -> 12% of each run, Pallas kernels for 0% -> 0%
where the time goes in v1:
time: 524 us
  waiting for transfers between devices  302 us (58%)
  blocking collectives  86.9 us (17%)
  matrix products  56.5 us (11%)
  starting transfers between devices  27.7 us (5%)
  other arithmetic  25.3 us (5%)
  between operations  13.8 us (3%)
  local copies, waits for them, and re-layouts  11.6 us (2%)
    ppermute x3, waiting for transfers between devices, ring_gather(): blocks.append(lax.ppermute(blocks[-1], axis, right))  97.1 us
    all_gather x1, blocking collectives, shards(): down_cols = lax.all_gather(down_scale, 'fs', axis=1, tiled=True)  74.9 us
    all_gather x1, waiting for transfers between devices, shards(): lax.all_gather(down_matrix.astype(jnp.bfloat16), 'fs', axis=1, tiled=True)  64.5 us
    reduce_scatter x1, waiting for transfers between devices, shards(): lax.psum_scatter(partial_ffn.astype(jnp.bfloat16), 'tp', scatter_dimensio...  42.8 us
    all_gather x1, waiting for transfers between devices, shards(): gathered = lax.all_gather(local_rows, 'tp', axis=1, tiled=True)  34.8 us
    all_gather x1, waiting for transfers between devices, shards(): lax.all_gather(in_matrix.astype(jnp.bfloat16), 'fs', axis=0, tiled=True)  26.5 us
    dot_general x1, matrix products, shards(): jnp.dot(hidden, lax.all_gather(down_matrix.astype(jnp.bfloat16), 'fs', ax...  23.9 us
    ppermute x3, starting transfers between devices, ring_gather(): blocks.append(lax.ppermute(blocks[-1], axis, right))  23.9 us
  transfers between devices with their start and end apart: 12, of which 9 were waited for; matrix products, arithmetic and copies ran while one was open for 12% of the time, Pallas kernels for 0%

profile of v1, /device:TPU:0, one launch (start us, length us, event | category | flops | bytes accessed | tf_op | source)
XLA Modules:
  0.0 523.8 jit_solution(16956328376864459134)
XLA Ops:
  11.3 34.8 %all-gather.21.cloned.1.call-done = bf16[1,1024,2048]{2,1,0:T(8,128)(2,1)} async-done(((bf16[1,1024,512]{2,1,0:T(8,128)(2,1)}), bf16[1,1024,2048]{2,1,0:T(8,128)(2,1)}) %all-gather.21.cloned.1.call-update) | async-done | bytes 4194320 | tf_op jit(solution)/shard_map/all_gather | solution.py:84
  46.1 3.1 fusion.3
  49.2 26.5 %all-gather.9.cloned.1.call-done = bf16[2048,256]{1,0:T(8,128)(2,1)} async-done(((bf16[512,256]{1,0:T(8,128)(2,1)}), bf16[2048,256]{1,0:T(8,128)(2,1)}) %all-gather.9.cloned.1.call-update) | async-done | bytes 1048592 | tf_op jit(solution)/shard_map/all_gather | solution.py:88
  75.7 3.8 fusion.20
  80.1 3.2 fusion.28
  84.4 20.3 %all-gather.13.cloned.1.call-done = bf16[256,2048]{0,1:T(8,128)(2,1)} async-done(((bf16[256,512]{0,1:T(8,128)(2,1)}), bf16[256,2048]{0,1:T(8,128)(2,1)}) %all-gather.13.cloned.1.call-update) | async-done | bytes 1048592 | tf_op jit(solution)/shard_map/all_gather | solution.py:107
  106.9 3.5 all-to-all-start
  110.5 11.9 %all_gather.31 = f32[1,2048]{1,0:T(1,128)S(1)} all-gather(f32[1,512]{1,0:T(1,128)S(1)} %copy-done.11), channel_id=1, replica_groups=mesh['grp'=2,'fs'=4,'tp'=4] {'fs'}, dimensions={1}, use_global_device_ids=true | all-gather | bytes 10240 | tf_op jit(solution)/shard_map/all_gather | solution.py:103
  122.5 12.5 %all-to-all-done = bf16[256,4,512]{2,0,1:T(8,128)(2,1)S(1)} async-done(((bf16[256,4,512]{2,0,1:T(8,128)(2,1)}), bf16[256,4,512]{2,0,1:T(8,128)(2,1)S(1)}, u32[]{:S(2)}, u32[]{:S(2)}) %all-to-all-start) | async-done | bytes 1048608 | tf_op jit(solution)/shard_map/all_to_all | solution.py:108
  135.0 2.7 all-gather.11.cloned.1.call-done
  137.6 3.0 multiply_convert_fusion.1
  142.7 3.1 convert_element_type.133
  150.0 33.0 %collective-permute-done = bf16[512,1408]{1,0:T(8,128)(2,1)} collective-permute-done((bf16[512,1408]{1,0:T(8,128)(2,1)}, bf16[512,1408]{1,0:T(8,128)(2,1)}, u32[]{:S(2)}, u32[]{:S(2)}) %collective-permute-start) | collective-permute-done | bytes 1441824 | tf_op jit(solution)/shard_map/ppermute | solution.py:22
  183.1 64.1 %collective-permute-done.1 = bf16[512,1408]{1,0:T(8,128)(2,1)} collective-permute-done((bf16[512,1408]{1,0:T(8,128)(2,1)}, bf16[512,1408]{1,0:T(8,128)(2,1)}, u32[]{:S(2)}, u32[]{:S(2)}) %collective-permute-start.1) | collective-permute-done | bytes 1441824 | tf_op jit(solution)/shard_map/ppermute | solution.py:22
  247.2 22.4 %collective-permute-start.2 = (bf16[512,1408]{1,0:T(8,128)(2,1)}, bf16[512,1408]{1,0:T(8,128)(2,1)}, u32[]{:S(2)}, u32[]{:S(2)}) collective-permute-start(bf16[512,1408]{1,0:T(8,128)(2,1)} %collective-permute-done.1), channel_id=1, source_target_pairs={{0,4},{4,8},{8,12},{12,0},{1,5},{5,9},{9,13},{13,1},{2,6},{6,10},{... | collective-permute-start | bytes 4325384 | tf_op jit(solution)/shard_map/ppermute | solution.py:22
  269.7 74.9 %all_gather.35 = f32[1,2048]{1,0:T(1,128)S(1)} all-gather(f32[1,512]{1,0:T(1,128)S(1)} %copy-done.12), channel_id=1, replica_groups=mesh['grp'=2,'fs'=4,'tp'=4] {'fs'}, dimensions={1}, use_global_device_ids=true | all-gather | bytes 10240 | tf_op jit(solution)/shard_map/all_gather | solution.py:134
  344.9 5.9 %pad_maximum_fusion = bf16[4,512,1408]{2,1,0:T(8,128)(2,1)} fusion(bf16[1,512,1408]{2,1,0:T(8,128)(2,1)} %bitcast.15, bf16[1,512,1408]{2,1,0:T(8,128)(2,1)} %bitcast.14, bf16[1,512,1408]{2,1,0:T(8,128)(2,1)} %bitcast.13, bf16[1,512,1408]{2,1,0:T(8,128)(2,1)S(1)} %convert_bitcast_fusion), kind=kLoop, calls=%fused_computation.14 | loop fusion | flops 8650752 | bytes 11534336 | tf_op jit(solution)/shard_map/stack | solution.py:24
  350.8 6.7 %gather_fusion = bf16[4,512,1408]{2,1,0:T(8,128)(2,1)} fusion(bf16[4,512,1408]{2,1,0:T(8,128)(2,1)} %pad_maximum_fusion, s32[1024]{0:T(1024)S(1)} %pad_clamp_fusion), kind=kCustom, calls=%fused_computation | custom fusion | bytes 11534352 | tf_op jit(solution)/shard_map/gather | solution.py:24
  357.5 3.1 fusion
  360.7 12.1 %fusion.11 = f32[1024,1408]{1,0:T(8,128)} fusion(bf16[2048,1408]{1,0:T(8,128)(2,1)} %all-gather.17.cloned.1.call-done, f32[1408]{0:T(1024)S(1)} %reduce.1, bf16[1024,2048]{1,0:T(8,128)(2,1)} %all-gather.15.cloned.1.call-done, f32[2048]{0:T(1024)S(1)} %copy-done.15, f32[1024]{0:T(1024)S(1)} %add_rsqrt_fusion), kind=kOutput, calls=%fused_computation.22 | convolution fusion | flops 5918294016 | bytes 15746560 | tf_op jit(solution)/shard_map/dot_general | solution.py:127
  372.7 10.5 %fusion.12 = f32[1024,1408]{1,0:T(8,128)} fusion(bf16[2048,1408]{1,0:T(8,128)(2,1)} %bitcast.89, f32[1408]{0:T(1024)S(1)} %reduce.5, bf16[1024,2048]{1,0:T(8,128)(2,1)S(1)} %copy-done.4, f32[2048]{0:T(1024)S(1)} %copy-done.15, f32[1024]{0:T(1024)S(1)} %add_rsqrt_fusion), kind=kOutput, calls=%fused_computation.23 | convolution fusion | flops 5918294016 | bytes 15746560 | tf_op jit(solution)/shard_map/dot_general | solution.py:128
  383.3 64.5 %all-gather.19.cloned.1.call-done = bf16[1408,2048]{1,0:T(8,128)(2,1)} async-done(((bf16[1408,512]{1,0:T(8,128)(2,1)}), bf16[1408,2048]{1,0:T(8,128)(2,1)}) %all-gather.19.cloned.1.call-update) | async-done | bytes 5767184 | tf_op jit(solution)/shard_map/all_gather | solution.py:138
  447.7 23.9 %multiply_convert_fusion = bf16[1024,2048]{1,0:T(8,128)(2,1)} fusion(bf16[1408,2048]{1,0:T(8,128)(2,1)} %all-gather.19.cloned.1.call-done, f32[2048]{0:T(1024)S(1)} %bitcast.92, f32[1022,1408]{1,0:T(8,128)} %bitcast.98, f32[1023,1408]{1,0:T(8,128)} %bitcast.99, f32[1024,1408]{1,0:T(8,128)} %fusion.12, f32[1022,1408]{1,0:T(8,128)} %bitcast.96, ...), kind=kOutput, calls=%fused_computation.11 | convolution fusion | flops 5932843008 | bytes 44572672 | tf_op jit(solution)/shard_map/dot_general | solution.py:136
  471.7 42.8 %reduce-scatter.2.cloned.1.call-done = bf16[1024,512]{1,0:T(8,128)(2,1)} async-done(((bf16[1024,2048]{1,0:T(8,128)(2,1)}), bf16[1024,512]{1,0:T(8,128)(2,1)}) %reduce-scatter.2.cloned.1.call-update) | async-done | bytes 1048592 | tf_op jit(solution)/shard_map/reduce_scatter | solution.py:143
  (85 shorter events, 17.6 us)
Async XLA Ops:
  6.5 73.6 %copy-start = (bf16[2,128,128]{2,1,0:T(8,128)(2,1)S(1)}, bf16[2,128,128]{2,1,0:T(8,128)(2,1)}, u32[]{:S(2)}) copy-start(bf16[2,128,128]{2,1,0:T(8,128)(2,1)} %param.21) | copy-start | bytes 196612
  6.5 69.2 %copy-start.16 = (f32[1,256]{1,0:T(1,128)S(1)}, f32[1,256]{1,0:T(1,128)}, u32[]{:S(2)}) copy-start(f32[1,256]{1,0:T(1,128)} %param.20) | copy-start | bytes 3076
  6.5 69.2 %copy-start.14 = (f32[2048]{0:T(1024)S(1)}, f32[2048]{0:T(1024)}, u32[]{:S(2)}) copy-start(f32[2048]{0:T(1024)} %param.18) | copy-start | bytes 24580
  6.5 39.6 %all-gather.21.cloned.1.call-start = ((), (), s32[]{:S(2)}) async-start(), calls=%async_computation.9 | async-start | bytes 5242880 | tf_op jit(solution)/shard_map/all_gather | solution.py:84
  7.3 68.4 %all-gather.9.cloned.1.call-start = ((), (), s32[]{:S(2)}) async-start(), calls=%async_computation.2 | async-start | bytes 1310720 | tf_op jit(solution)/shard_map/all_gather | solution.py:88
  9.1 95.6 %all-gather.13.cloned.1.call-start = ((), (), s32[]{:S(2)}) async-start(), calls=%async_computation.4 | async-start | bytes 1310720 | tf_op jit(solution)/shard_map/all_gather | solution.py:107
  11.1 126.6 %all-gather.11.cloned.1.call-start = ((), (), s32[]{:S(2)}) async-start(), calls=%async_computation.3 | async-start | bytes 2621440 | tf_op jit(solution)/shard_map/all_gather | solution.py:106
  83.4 27.1 %copy-start.11 = (f32[1,512]{1,0:T(1,128)S(1)}, f32[1,512]{1,0:T(1,128)}, u32[]{:S(2)}) copy-start(f32[1,512]{1,0:T(1,128)} %param.24) | copy-start | bytes 6148
  106.9 28.0 %all-to-all-start = ((bf16[256,4,512]{2,0,1:T(8,128)(2,1)}), bf16[256,4,512]{2,0,1:T(8,128)(2,1)S(1)}, u32[]{:S(2)}, u32[]{:S(2)}) async-start(bf16[256,4,512]{2,0,1:T(8,128)(2,1)} %copy.23), calls=%async_computation | async-start | bytes 2097152 | tf_op jit(solution)/shard_map/all_to_all | solution.py:108
  110.5 247.1 %all-gather.15.cloned.1.call-start = ((), (), s32[]{:S(2)}) async-start(), calls=%async_computation.5 | async-start | bytes 5242880 | tf_op jit(solution)/shard_map/all_gather | solution.py:119
  142.6 218.0 %all-gather.17.cloned.1.call-start = ((), (), s32[]{:S(2)}) async-start(), calls=%async_computation.6 | async-start | bytes 7208960 | tf_op jit(solution)/shard_map/all_gather | solution.py:124
  145.8 123.8 %copy-start.9 = (f32[1,1408]{1,0:T(1,128)S(1)}, f32[1,1408]{1,0:T(1,128)}, u32[]{:S(2)}) copy-start(f32[1,1408]{1,0:T(1,128)} %param.27) | copy-start | bytes 16900
  145.8 123.8 %copy-start.10 = (f32[1,1408]{1,0:T(1,128)S(1)}, f32[1,1408]{1,0:T(1,128)}, u32[]{:S(2)}) copy-start(f32[1,1408]{1,0:T(1,128)} %param.29) | copy-start | bytes 16900
  145.8 123.8 %copy-start.12 = (f32[1,512]{1,0:T(1,128)S(1)}, f32[1,512]{1,0:T(1,128)}, u32[]{:S(2)}) copy-start(f32[1,512]{1,0:T(1,128)} %param.33) | copy-start | bytes 6148
  145.8 198.8 %copy-start.7 = (f32[3,1408]{1,0:T(4,128)S(1)}, f32[3,1408]{1,0:T(4,128)}, u32[]{:S(2)}) copy-start(f32[3,1408]{1,0:T(4,128)} %param.31) | copy-start | bytes 50692
  145.8 198.8 %copy-start.8 = (f32[3,1408]{1,0:T(4,128)S(1)}, f32[3,1408]{1,0:T(4,128)}, u32[]{:S(2)}) copy-start(f32[3,1408]{1,0:T(4,128)} %param.30) | copy-start | bytes 50692
  145.9 301.8 %all-gather.19.cloned.1.call-start = ((), (), s32[]{:S(2)}) async-start(), calls=%async_computation.7 | async-start | bytes 7208960 | tf_op jit(solution)/shard_map/all_gather | solution.py:138
  147.2 35.8 %collective-permute-start = (bf16[512,1408]{1,0:T(8,128)(2,1)}, bf16[512,1408]{1,0:T(8,128)(2,1)}, u32[]{:S(2)}, u32[]{:S(2)}) collective-permute-start(bf16[512,1408]{1,0:T(8,128)(2,1)} %convert_element_type.136), channel_id=1, source_target_pairs={{0,4},{4,8},{8,12},{12,0},{1,5},{5,9},{9,13},{13,1},{2,6},{6,10},{... | collective-permute-start | bytes 4325384 | tf_op jit(solution)/shard_map/ppermute | solution.py:22
  150.0 364.5 %reduce-scatter.2.cloned.1.call-start = ((), (), s32[]{:S(2)}) async-start(), calls=%async_computation.8 | async-start | bytes 5242880 | tf_op jit(solution)/shard_map/reduce_scatter | solution.py:143
  183.1 64.1 %collective-permute-start.1 = (bf16[512,1408]{1,0:T(8,128)(2,1)}, bf16[512,1408]{1,0:T(8,128)(2,1)}, u32[]{:S(2)}, u32[]{:S(2)}) collective-permute-start(bf16[512,1408]{1,0:T(8,128)(2,1)} %collective-permute-done), channel_id=1, source_target_pairs={{0,4},{4,8},{8,12},{12,0},{1,5},{5,9},{9,13},{13,1},{2,6},{6,10},{... | collective-permute-start | bytes 4325384 | tf_op jit(solution)/shard_map/ppermute | solution.py:22
  247.2 97.7 %collective-permute-start.2 = (bf16[512,1408]{1,0:T(8,128)(2,1)}, bf16[512,1408]{1,0:T(8,128)(2,1)}, u32[]{:S(2)}, u32[]{:S(2)}) collective-permute-start(bf16[512,1408]{1,0:T(8,128)(2,1)} %collective-permute-done.1), channel_id=1, source_target_pairs={{0,4},{4,8},{8,12},{12,0},{1,5},{5,9},{9,13},{13,1},{2,6},{6,10},{... | collective-permute-start | bytes 4325384 | tf_op jit(solution)/shard_map/ppermute | solution.py:22
  360.7 12.1 %copy-start.4 = (bf16[1024,2048]{1,0:T(8,128)(2,1)S(1)}, bf16[1024,2048]{1,0:T(8,128)(2,1)}, u32[]{:S(2)}) copy-start(bf16[1024,2048]{1,0:T(8,128)(2,1)} %all-gather.15.cloned.1.call-done) | copy-start | bytes 12582916
  447.7 66.8 %copy-start.3 = (bf16[1024,512]{1,0:T(8,128)(2,1)S(1)}, bf16[1024,512]{1,0:T(8,128)(2,1)}, u32[]{:S(2)}) copy-start(bf16[1024,512]{1,0:T(8,128)(2,1)} %fusion.13) | copy-start | bytes 3145732
  447.7 69.2 %copy-start.1 = (bf16[2,128,128]{2,1,0:T(8,128)(2,1)S(1)}, bf16[2,128,128]{2,1,0:T(8,128)(2,1)}, u32[]{:S(2)}) copy-start(bf16[2,128,128]{2,1,0:T(8,128)(2,1)} %param.21) | copy-start | bytes 196612
  (5 other events, 24.1 us)
Sparse Core Ops, SparseCore 0:
  8.9 37.1 all-gather.20
  47.7 27.9 all-gather.8
  77.3 27.3 all-gather.12
  106.1 31.4 all-gather.10
  142.8 32.9 all-gather.14
  177.1 164.9 all-gather.16
  343.7 103.9 all-gather.18
  471.8 42.6 reduce-scatter.1
